TPU v7x, 32 devices: a whole 2x2x4 slice. The times are simulated.
32 devices in a mesh: fs: 8 (over z, y), tp: 4 (over x, core).
Axes of the slice: x: 2, y: 2, z: 4, core: 2. Of those that a mesh axis runs over, the one named last changes fastest.
Arguments:
- prompt: bfloat16 [4096, 2048], P(('fs', 'tp')), may hold values from -6 to 6
- norm_gain: float32 [2048], P('fs'), may hold values from 0.1 to 1.9
- up_trained: float32 [2048, 8192], P('fs', 'tp'), may hold values from -0.125 to 0.125
- down_trained: float32 [2048, 8192], P('fs', 'tp'), may hold values from -0.0625 to 0.0625
Outputs:
- up_served: bfloat16 [2048, 8192], P(None, 'tp')
- down_served: bfloat16 [8192, 2048], P('tp')
- mixed: bfloat16 [4096, 2048], P(('fs', 'tp'))
All inputs are finite; a program needn't handle non-finite values.
Results may differ from a plain program's by a relative error of at most 0.014.
Values may be sent and summed in bfloat16 or wider, within the bound.
A program may use at most 128 MiB of HBM per device.

v0:
```python
import jax
import jax.numpy as jnp
from jax import lax
from jax.sharding import PartitionSpec as P


def shards(prompt, norm_gain, up_trained, down_trained):
    up_local = (norm_gain[:, None] * up_trained).astype(jnp.bfloat16)
    down_local = down_trained.astype(jnp.bfloat16)
    values = prompt.astype(jnp.float32)
    scale = lax.rsqrt(jnp.mean(values * values, axis=-1, keepdims=True) + 1e-06)
    normed = (values * scale).astype(jnp.bfloat16)
    group_rows = lax.all_gather(normed, "tp", axis=0, tiled=True)
    pieces = (
        lax.all_gather(up_local, "fs", axis=0, tiled=True),
        lax.all_gather(down_local, "fs", axis=0, tiled=True),
    )
    pre = jnp.dot(group_rows, pieces[0], preferred_element_type=jnp.float32)
    up_buffer = pieces[0]
    down_buffer = pieces[1]
    pre, up_whole, down_whole = (pre, up_buffer, down_buffer)
    hidden = jnp.square(jax.nn.relu(pre)).astype(jnp.bfloat16)
    down_served = jnp.transpose(down_whole)
    mixed = lax.psum_scatter(
        jnp.dot(hidden, down_served, preferred_element_type=jnp.float32).astype(jnp.bfloat16),
        "tp",
        scatter_dimension=0,
        tiled=True,
    )
    return (up_whole, down_served, mixed)


def solution(mesh):
    return jax.shard_map(
        shards,
        mesh=mesh,
        in_specs=(P(("fs", "tp"), None), P("fs"), P("fs", "tp"), P("fs", "tp")),
        out_specs=(P(None, "tp"), P("tp", None), P(("fs", "tp"), None)),
        check_vma=False,
    )
```

profile of v0, /device:TPU:0, one launch (start us, length us, event | category | flops | bytes accessed | tf_op | source)
XLA Modules:
  0.0 358.5 jit_solution(13753829205279300968)
XLA Ops:
  7.2 0.0 copy-start
  7.2 0.0 all-gather.8.cloned.1.call-start
  7.2 1.4 fusion
  8.6 2.0 fusion.1
  10.6 0.0 all-gather.8.cloned.1.call-update
  10.6 0.0 all-gather.4.cloned.1.call-start
  10.7 2.7 multiply_convert_fusion.1
  13.4 0.0 all-gather.4.cloned.1.call-update
  13.4 0.0 all-gather.6.cloned.1.call-start
  13.5 0.0 copy-done
  13.5 1.4 copy.7
  14.9 0.0 all-gather.6.cloned.1.call-update
  14.9 0.0 reduce-scatter.2.cloned.1.call-start
  14.9 21.1 %all-gather.8.cloned.1.call-done = bf16[512,2048]{1,0:T(8,128)(2,1)} async-done(((bf16[128,2048]{1,0:T(8,128)(2,1)}), bf16[512,2048]{1,0:T(8,128)(2,1)}) %all-gather.8.cloned.1.call-update) | async-done | bytes 2097168 | tf_op jit(solution)/shard_map/all_gather | solution.py:13
  36.1 127.2 %all-gather.4.cloned.1.call-done = bf16[2048,2048]{1,0:T(8,128)(2,1)} async-done(((bf16[256,2048]{1,0:T(8,128)(2,1)}), bf16[2048,2048]{1,0:T(8,128)(2,1)}) %all-gather.4.cloned.1.call-update) | async-done | bytes 8388624 | tf_op jit(solution)/shard_map/all_gather | solution.py:15
  163.3 125.8 %all-gather.6.cloned.1.call-done = bf16[2048,2048]{0,1:T(8,128)(2,1)} async-done(((bf16[256,2048]{0,1:T(8,128)(2,1)}), bf16[2048,2048]{0,1:T(8,128)(2,1)}) %all-gather.6.cloned.1.call-update) | async-done | bytes 8388624 | tf_op jit(solution)/shard_map/all_gather | solution.py:16
  289.0 16.5 %convolution_convert_fusion = bf16[512,2048]{1,0:T(8,128)(2,1)} fusion(bf16[2048,2048]{0,1:T(8,128)(2,1)} %all-gather.6.cloned.1.call-done, bf16[512,2048]{1,0:T(8,128)(2,1)} %all-gather.8.cloned.1.call-done, bf16[2048,2048]{1,0:T(8,128)(2,1)} %all-gather.4.cloned.1.call-done), kind=kOutput, calls=%fused_computation.1 | convolution fusion | flops 8594128896 | bytes 20971520 | tf_op jit(solution)/shard_map/dot_general | solution.py:25
  305.5 0.0 reduce-scatter.2.cloned.1.call-update
  305.6 29.5 %reduce-scatter.2.cloned.1.call-done = bf16[128,2048]{1,0:T(8,128)(2,1)} async-done(((bf16[512,2048]{1,0:T(8,128)(2,1)}), bf16[128,2048]{1,0:T(8,128)(2,1)}) %reduce-scatter.2.cloned.1.call-update) | async-done | bytes 524304 | tf_op jit(solution)/shard_map/reduce_scatter | solution.py:24
  335.0 8.4 %copy.10 = bf16[2048,2048]{1,0:T(8,128)(2,1)} copy(bf16[2048,2048]{1,0:T(8,128)(2,1)} %all-gather.4.cloned.1.call-done) | data formatting | bytes 16777216
  343.5 8.4 %copy.11 = bf16[2048,2048]{1,0:T(8,128)(2,1)} copy(bf16[2048,2048]{1,0:T(8,128)(2,1)} %bitcast.4) | data formatting | bytes 16777216
  (1 shorter events, 0.0 us)
Async XLA Ops:
  7.2 6.3 %copy-start = (f32[256,2048]{1,0:T(8,128)S(1)}, f32[256,2048]{1,0:T(8,128)}, u32[]{:S(2)}) copy-start(f32[256,2048]{1,0:T(8,128)} %param.7) | copy-start | bytes 6291460
  7.2 28.9 %all-gather.8.cloned.1.call-start = ((), (), s32[]{:S(2)}) async-start(), calls=%async_computation.3 | async-start | bytes 2621440 | tf_op jit(solution)/shard_map/all_gather | solution.py:13
  10.6 152.6 %all-gather.4.cloned.1.call-start = ((), (), s32[]{:S(2)}) async-start(), calls=%async_computation.1 | async-start | bytes 9437184 | tf_op jit(solution)/shard_map/all_gather | solution.py:15
  13.4 275.6 %all-gather.6.cloned.1.call-start = ((), (), s32[]{:S(2)}) async-start(), calls=%async_computation.2 | async-start | bytes 9437184 | tf_op jit(solution)/shard_map/all_gather | solution.py:16
  14.9 320.2 %reduce-scatter.2.cloned.1.call-start = ((), (), s32[]{:S(2)}) async-start(), calls=%async_computation.4 | async-start | bytes 2621440 | tf_op jit(solution)/shard_map/reduce_scatter | solution.py:24
Sparse Core Ops, SparseCore 0:
  10.7 25.2 all-gather.7
  38.8 124.4 all-gather.3
  165.9 123.1 all-gather.5
  305.7 29.3 reduce-scatter.1
where the time goes:
time: 359 us; the launch traced here: 358 us
  waiting for transfers between devices  304 us (85%)
  local copies, waits for them, and re-layouts  18.3 us (5%)
  matrix products  16.5 us (5%)
  between operations  13.8 us (4%)
  other arithmetic  6.11 us (2%)
    all_gather x1, waiting for transfers between devices, shards(): lax.all_gather(up_local, 'fs', axis=0, tiled=True)  127 us
    all_gather x1, waiting for transfers between devices, shards(): lax.all_gather(down_local, 'fs', axis=0, tiled=True)  126 us
    reduce_scatter x1, waiting for transfers between devices, shards(): lax.psum_scatter(jnp.dot(hidden, down_served, preferred_element_type=jnp....  29.5 us
    all_gather x1, waiting for transfers between devices, shards(): group_rows = lax.all_gather(normed, 'tp', axis=0, tiled=True)  21.1 us
    unnamed x5, local copies, waits for them, and re-layouts  18.3 us
    dot_general x1, matrix products, shards(): jnp.dot(hidden, down_served, preferred_element_type=jnp.float32)  16.5 us
  transfers between devices with their start and end apart: 4, of which 4 were waited for; matrix products, arithmetic and copies ran while one was open for 1% of the time, Pallas kernels for 0%

commit v1 on v0

--- a/solution.py
+++ b/solution.py
@@ -10,7 +10,12 @@
     values = prompt.astype(jnp.float32)
     scale = lax.rsqrt(jnp.mean(values * values, axis=-1, keepdims=True) + 1e-06)
     normed = (values * scale).astype(jnp.bfloat16)
-    group_rows = lax.all_gather(normed, "tp", axis=0, tiled=True)
+    ring = [normed]
+    for hop in range(3):
+        ring.append(lax.ppermute(ring[-1], "tp", [(dev, (dev + 1) % 4) for dev in range(4)]))
+    group_rows = jnp.roll(
+        jnp.concatenate(ring[::-1], axis=0), (lax.axis_index("tp") + 1) * ring[0].shape[0], axis=0
+    )
     pieces = (
         lax.all_gather(up_local, "fs", axis=0, tiled=True),
         lax.all_gather(down_local, "fs", axis=0, tiled=True),

time: 359 us -> 333 us (0.928)
  waiting for transfers between devices: 304 us -> 273 us
  local copies, waits for them, and re-layouts: 18.3 us -> 23.2 us
    all_gather x1, waiting for transfers between devices: 127 us -> 92.5 us  [shards(): lax.all_gather(up_local, 'fs', axis=0, tiled=True)]
    ppermute x0 -> x3, waiting for transfers between devices: none -> 26 us  [shards(): lax.ppermute(ring[-1], 'tp', [(dev, (dev + 1) % 4) for dev in range(4)])]
    all_gather x1 -> x0, waiting for transfers between devices: 21.1 us -> none  [shards(): group_rows = lax.all_gather(normed, 'tp', axis=0, tiled=True)]
    unnamed x5 -> x13, local copies, waits for them, and re-layouts: 18.3 us -> 23.2 us
  transfers between devices with their start and end apart: 4 -> 6, of which waited for: 4 -> 6; matrix products, arithmetic and copies ran while one was open for 1% -> 3% of each run, Pallas kernels for 0% -> 0%
where the time goes in v1:
time: 333 us
  waiting for transfers between devices  273 us (82%)
  local copies, waits for them, and re-layouts  23.2 us (7%)
  matrix products  16.5 us (5%)
  between operations  13.8 us (4%)
  other arithmetic  5.14 us (2%)
    all_gather x1, waiting for transfers between devices, shards(): lax.all_gather(down_local, 'fs', axis=0, tiled=True)  125 us
    all_gather x1, waiting for transfers between devices, shards(): lax.all_gather(up_local, 'fs', axis=0, tiled=True)  92.5 us
    reduce_scatter x1, waiting for transfers between devices, shards(): lax.psum_scatter(jnp.dot(hidden, down_served, preferred_element_type=jnp....  29.5 us
    ppermute x3, waiting for transfers between devices, shards(): lax.ppermute(ring[-1], 'tp', [(dev, (dev + 1) % 4) for dev in range(4)])  26 us
    unnamed x13, local copies, waits for them, and re-layouts  23.2 us
    dot_general x1, matrix products, shards(): jnp.dot(hidden, down_served, preferred_element_type=jnp.float32)  16.5 us
  transfers between devices with their start and end apart: 6, of which 6 were waited for; matrix products, arithmetic and copies ran while one was open for 3% of the time, Pallas kernels for 0%

profile of v1, /device:TPU:0, one launch (start us, length us, event | category | flops | bytes accessed | tf_op | source)
XLA Modules:
  0.0 332.5 jit_solution(10200360888882709802)
XLA Ops:
  7.2 0.0 copy-start.1
  7.2 0.0 copy-start
  7.2 0.0 all-gather.3.cloned.1.call-start
  7.2 2.9 multiply_convert_fusion.1
  10.1 0.0 all-gather.3.cloned.1.call-update
  10.1 0.0 all-gather.5.cloned.1.call-start
  10.2 0.0 copy-done.1
  10.2 1.4 copy.7
  11.6 0.0 all-gather.5.cloned.1.call-update
  11.6 0.0 reduce-scatter.2.cloned.1.call-start
  11.7 0.0 copy-done
  11.7 0.2 fusion.1
  11.9 0.2 fusion.2
  12.0 0.5 collective-permute-start
  12.6 8.8 %collective-permute-done = bf16[128,2048]{1,0:T(8,128)(2,1)S(1)} collective-permute-done((bf16[128,2048]{1,0:T(8,128)(2,1)S(1)}, bf16[128,2048]{1,0:T(8,128)(2,1)S(1)}, u32[]{:S(2)}, u32[]{:S(2)}) %collective-permute-start) | collective-permute-done | bytes 524320 | tf_op jit(solution)/shard_map/ppermute | solution.py:15
  21.4 0.0 collective-permute-start.1
  21.4 8.6 %collective-permute-done.1 = bf16[128,2048]{1,0:T(8,128)(2,1)S(1)} collective-permute-done((bf16[128,2048]{1,0:T(8,128)(2,1)S(1)}, bf16[128,2048]{1,0:T(8,128)(2,1)S(1)}, u32[]{:S(2)}, u32[]{:S(2)}) %collective-permute-start.1) | collective-permute-done | bytes 524320 | tf_op jit(solution)/shard_map/ppermute | solution.py:15
  30.0 0.0 collective-permute-start.2
  30.0 8.6 %collective-permute-done.2 = bf16[128,2048]{1,0:T(8,128)(2,1)S(1)} collective-permute-done((bf16[128,2048]{1,0:T(8,128)(2,1)S(1)}, bf16[128,2048]{1,0:T(8,128)(2,1)S(1)}, u32[]{:S(2)}, u32[]{:S(2)}) %collective-permute-start.2) | collective-permute-done | bytes 524320 | tf_op jit(solution)/shard_map/ppermute | solution.py:15
  38.6 0.8 constant_dynamic-update-slice_fusion.7
  39.4 0.8 constant_dynamic-update-slice_fusion.6
  40.2 0.8 constant_dynamic-update-slice_fusion.5
  41.1 0.9 constant_dynamic-update-slice_fusion.4
  42.0 0.8 constant_dynamic-update-slice_fusion.3
  42.8 0.8 constant_dynamic-update-slice_fusion.2
  43.7 0.8 constant_dynamic-update-slice_fusion.1
  44.5 0.9 constant_dynamic-update-slice_fusion
  45.4 92.5 %all-gather.3.cloned.1.call-done = bf16[2048,2048]{1,0:T(8,128)(2,1)} async-done(((bf16[256,2048]{1,0:T(8,128)(2,1)}), bf16[2048,2048]{1,0:T(8,128)(2,1)}) %all-gather.3.cloned.1.call-update) | async-done | bytes 8388624 | tf_op jit(solution)/shard_map/all_gather | solution.py:20
  137.9 125.2 %all-gather.5.cloned.1.call-done = bf16[2048,2048]{0,1:T(8,128)(2,1)} async-done(((bf16[256,2048]{0,1:T(8,128)(2,1)}), bf16[2048,2048]{0,1:T(8,128)(2,1)}) %all-gather.5.cloned.1.call-update) | async-done | bytes 8388624 | tf_op jit(solution)/shard_map/all_gather | solution.py:21
  263.1 16.5 %convolution_convert_fusion = bf16[512,2048]{1,0:T(8,128)(2,1)} fusion(bf16[2048,2048]{0,1:T(8,128)(2,1)} %all-gather.5.cloned.1.call-done, bf16[2048,2048]{1,0:T(8,128)(2,1)} %all-gather.3.cloned.1.call-done, bf16[1024,2048]{1,0:T(8,128)(2,1)} %constant_dynamic-update-slice_fusion, s32[]{:T(128)S(6)} %select_n.14), kind=kOutput, calls=%fused_computation.1 | convolution fusion | flops 8594128896 | bytes 20971524 | tf_op jit(solution)/shard_map/dot_general | solution.py:30
  279.6 0.0 reduce-scatter.2.cloned.1.call-update
  279.6 29.5 %reduce-scatter.2.cloned.1.call-done = bf16[128,2048]{1,0:T(8,128)(2,1)} async-done(((bf16[512,2048]{1,0:T(8,128)(2,1)}), bf16[128,2048]{1,0:T(8,128)(2,1)}) %reduce-scatter.2.cloned.1.call-update) | async-done | bytes 524304 | tf_op jit(solution)/shard_map/reduce_scatter | solution.py:29
  309.1 8.4 %copy.17 = bf16[2048,2048]{1,0:T(8,128)(2,1)} copy(bf16[2048,2048]{1,0:T(8,128)(2,1)} %all-gather.3.cloned.1.call-done) | data formatting | bytes 16777216
  317.6 8.4 %copy.18 = bf16[2048,2048]{1,0:T(8,128)(2,1)} copy(bf16[2048,2048]{1,0:T(8,128)(2,1)} %bitcast.8) | data formatting | bytes 16777216
  (1 shorter events, 0.0 us)
Async XLA Ops:
  7.2 3.0 copy-start.1
  7.2 4.5 %copy-start = (bf16[128,2048]{1,0:T(8,128)(2,1)S(1)}, bf16[128,2048]{1,0:T(8,128)(2,1)}, u32[]{:S(2)}) copy-start(bf16[128,2048]{1,0:T(8,128)(2,1)} %param.4) | copy-start | bytes 1572868
  7.2 130.7 %all-gather.3.cloned.1.call-start = ((), (), s32[]{:S(2)}) async-start(), calls=%async_computation.1 | async-start | bytes 9437184 | tf_op jit(solution)/shard_map/all_gather | solution.py:20
  10.1 253.0 %all-gather.5.cloned.1.call-start = ((), (), s32[]{:S(2)}) async-start(), calls=%async_computation.2 | async-start | bytes 9437184 | tf_op jit(solution)/shard_map/all_gather | solution.py:21
  11.6 297.5 %reduce-scatter.2.cloned.1.call-start = ((), (), s32[]{:S(2)}) async-start(), calls=%async_computation.3 | async-start | bytes 2621440 | tf_op jit(solution)/shard_map/reduce_scatter | solution.py:29
  12.0 9.3 %collective-permute-start = (bf16[128,2048]{1,0:T(8,128)(2,1)S(1)}, bf16[128,2048]{1,0:T(8,128)(2,1)S(1)}, u32[]{:S(2)}, u32[]{:S(2)}) collective-permute-start(bf16[128,2048]{1,0:T(8,128)(2,1)S(1)} %fusion.2), channel_id=1, source_target_pairs={{0,1},{1,2},{2,3},{3,0},{4,5},{5,6},{6,7},{7,4},{8,9},{9,10},{10,1... | collective-permute-start | bytes 1572872 | tf_op jit(solution)/shard_map/ppermute | solution.py:15
  21.4 8.6 %collective-permute-start.1 = (bf16[128,2048]{1,0:T(8,128)(2,1)S(1)}, bf16[128,2048]{1,0:T(8,128)(2,1)S(1)}, u32[]{:S(2)}, u32[]{:S(2)}) collective-permute-start(bf16[128,2048]{1,0:T(8,128)(2,1)S(1)} %collective-permute-done), channel_id=1, source_target_pairs={{0,1},{1,2},{2,3},{3,0},{4,5},{5,6},{6,7},{7,4},{8,9},{9,10},{10,1... | collective-permute-start | bytes 1572872 | tf_op jit(solution)/shard_map/ppermute | solution.py:15
  30.0 8.6 %collective-permute-start.2 = (bf16[128,2048]{1,0:T(8,128)(2,1)S(1)}, bf16[128,2048]{1,0:T(8,128)(2,1)S(1)}, u32[]{:S(2)}, u32[]{:S(2)}) collective-permute-start(bf16[128,2048]{1,0:T(8,128)(2,1)S(1)} %collective-permute-done.1), channel_id=1, source_target_pairs={{0,1},{1,2},{2,3},{3,0},{4,5},{5,6},{6,7},{7,4},{8,9},{9,10},{10,1... | collective-permute-start | bytes 1572872 | tf_op jit(solution)/shard_map/ppermute | solution.py:15
Sparse Core Ops, SparseCore 0:
  10.7 127.1 all-gather.2
  140.0 123.1 all-gather.4
  279.8 29.3 reduce-scatter.1
